TPU v7x, 128 devices: a whole 4x4x4 slice. The times are simulated.
128 devices in a mesh: ep: 128 (over z, y, x, core).
Axes of the slice: x: 4, y: 4, z: 4, core: 2. Of those that a mesh axis runs over, the one named last changes fastest.
Arguments:
- tokens: bfloat16 [16384, 2048], P('ep'), may hold values from -6 to 6
- norm_gain: float32 [2048], replicated, may hold values from 0.1 to 1.9
- expert_ids: int32 [16384, 4], P('ep'), may hold values from 0 to 255, as said below
- gate_weights: float32 [16384, 4], P('ep'), may hold values from 0.1 to 0.6
- expert_gate: bfloat16 [256, 2048, 512], P('ep'), may hold values from -0.125 to 0.125
- expert_up: bfloat16 [256, 2048, 512], P('ep'), may hold values from -0.125 to 0.125
- expert_down: bfloat16 [256, 512, 2048], P('ep'), may hold values from -0.25 to 0.25
- shared_gate: bfloat16 [2048, 512], P('ep'), may hold values from -0.125 to 0.125
- shared_up: bfloat16 [2048, 512], P('ep'), may hold values from -0.125 to 0.125
- shared_down: bfloat16 [512, 2048], P(None, 'ep'), may hold values from -0.25 to 0.25
Outputs:
- mixed: bfloat16 [16384, 2048], P('ep')
Inputs may be any that keep to these rules, and one draw needn't show every extreme that they name: `expert_ids`: expert e belongs to device e // 2; each row names 4 experts of 4 different devices; among the rows of one device at most 6 name experts of any one device, hence at most 6 any one expert; in every aligned block of 128 rows exactly 6 rows name one and the same expert.
All inputs are finite; a program needn't handle non-finite values.
Results may differ from a plain program's by a relative error of at most 0.0067.
Values may be sent and summed in bfloat16 or wider, within the bound.
A program may use at most 128 MiB of HBM per device.

v0:
```python
import jax
import jax.numpy as jnp
from jax import lax
from jax.sharding import PartitionSpec as P

EPS = 1e-06


def side_by_side(arrays, axis, dim, along):
    both = jnp.concatenate(arrays, axis=along)
    out, at, outs = (lax.all_gather(both, axis, axis=dim, tiled=True), 0, [])
    for a in arrays:
        outs.append(lax.slice_in_dim(out, at, at + a.shape[along], axis=along))
        at += a.shape[along]
    return tuple(outs)


def normalize(tokens, norm_gain):
    values = tokens.astype(jnp.float32)
    scaled = values * lax.rsqrt(jnp.mean(values * values, axis=-1, keepdims=True) + EPS)
    return (scaled * norm_gain).astype(jnp.bfloat16)


def run_single(w_gate, w_up, w_down, incoming):
    gate_val = jnp.einsum("scd,df->scf", incoming, w_gate, preferred_element_type=jnp.float32)
    up_val = jnp.einsum("scd,df->scf", incoming, w_up, preferred_element_type=jnp.float32)
    hidden = (jax.nn.silu(gate_val) * up_val).astype(jnp.bfloat16)
    return jnp.einsum("scf,fd->scd", hidden, w_down, preferred_element_type=jnp.float32).astype(
        jnp.bfloat16
    )


def run_packed(w_gate, w_up, w_down, incoming):
    rows, which = incoming
    result = jnp.zeros(rows.shape, jnp.bfloat16)
    for local in range(w_gate.shape[0]):
        output = run_single(w_gate[local], w_up[local], w_down[local], rows)
        result = jnp.where((which == local)[:, :, None], output, result)
    return result


def per_device(
    tokens,
    norm_gain,
    expert_ids,
    gate_weights,
    expert_gate,
    expert_up,
    expert_down,
    shared_gate,
    shared_up,
    shared_down,
):
    normed = normalize(tokens, norm_gain)
    count_tok, top = expert_ids.shape
    width = normed.shape[1]
    local_experts = expert_gate.shape[0]
    devices_ep = lax.axis_size("ep")
    mean_rows = count_tok * top // devices_ep
    capacity = mean_rows + mean_rows // 2
    flat_ids = expert_ids.reshape(count_tok * top)
    copies = jnp.repeat(normed, top, axis=0)
    target = flat_ids // local_experts
    one_hot = (target[:, None] == jnp.arange(devices_ep, dtype=jnp.int32)[None, :]).astype(
        jnp.int32
    )
    running = jnp.cumsum(one_hot, axis=0)
    slot_index = jnp.sum(running * one_hot, axis=1) - 1
    position = target * capacity + slot_index
    outgoing = jnp.zeros((devices_ep * capacity, width), jnp.bfloat16).at[position].set(copies)
    labels = (
        jnp.full((devices_ep * capacity,), -1, jnp.int32).at[position].set(flat_ids % local_experts)
    )
    outgoing = outgoing.reshape(devices_ep, capacity, width)
    labels = labels.reshape(devices_ep, capacity)
    results = run_packed(
        expert_gate,
        expert_up,
        expert_down,
        (
            lax.all_to_all(outgoing, "ep", split_axis=0, concat_axis=0, tiled=True),
            lax.all_to_all(labels, "ep", split_axis=0, concat_axis=0, tiled=True),
        ),
    )
    returned = lax.all_to_all(results, "ep", split_axis=0, concat_axis=0, tiled=True)
    returned = returned.reshape(devices_ep * capacity, width)
    picked = returned[position].reshape(count_tok, top, width)
    routed = jnp.sum(picked.astype(jnp.float32) * gate_weights[:, :, None], axis=1)
    pieces = side_by_side((shared_gate, shared_up), "ep", 0, 1)
    gate_val = jnp.dot(normed, pieces[0], preferred_element_type=jnp.float32)
    up_val = jnp.dot(normed, pieces[1], preferred_element_type=jnp.float32)
    shared_hidden = (jax.nn.silu(gate_val) * up_val).astype(jnp.bfloat16)
    shared = jnp.dot(
        shared_hidden,
        lax.all_gather(shared_down, "ep", axis=1, tiled=True),
        preferred_element_type=jnp.float32,
    )
    return (routed + shared).astype(jnp.bfloat16)


def solution(mesh):
    return jax.shard_map(
        per_device,
        mesh=mesh,
        in_specs=(
            P("ep", None),
            P(),
            P("ep", None),
            P("ep", None),
            P("ep", None, None),
            P("ep", None, None),
            P("ep", None, None),
            P("ep", None),
            P("ep", None),
            P(None, "ep"),
        ),
        out_specs=P("ep", None),
        check_vma=False,
    )
```

profile of v0, /device:TPU:1, one launch (start us, length us, event | category | flops | bytes accessed | tf_op | source)
XLA Modules:
  0.0 233.6 jit_solution(13163270796150500053)
XLA Ops:
  6.5 0.0 copy-start.2
  6.5 0.0 all-gather.3.cloned.1.call-start
  6.5 1.4 pad_maximum_fusion
  8.0 0.0 all-gather.3.cloned.1.call-update
  8.0 0.8 copy.36
  8.8 0.1 reshape.172
  8.9 0.1 reshape.171
  9.0 0.1 reshape.170
  9.1 0.1 copy.39
  9.2 0.2 fusion.55
  9.6 0.2 fusion.49
  9.8 2.4 %scatter_custom_fusion = s32[768]{0:T(1024)S(1)} fusion(s32[512]{0:T(512)S(1)} %bitcast.56, s32[512]{0:T(512)S(1)} %get-tuple-element.7, s32[]{:T(128)} %constant.46.clone.1), kind=kCustom, calls=%fused_computation.81 | custom fusion | bytes 3076 | tf_op jit(solution)/shard_map/scatter | solution.py:72
  12.3 0.8 all_to_all.12
  13.0 11.5 %all-to-all-start = ((s32[128,1,6]{2,1,0:T(1,128)}), s32[128,1,6]{2,1,0:T(1,128)S(1)}, u32[]{:S(2)}, u32[]{:S(2)}) async-start(s32[128,1,6]{2,1,0:T(1,128)} %bitcast.5), calls=%async_computation | async-start | bytes 131072 | tf_op jit(solution)/shard_map/all_to_all | solution.py:82
  24.5 1.2 fusion.35
  25.8 0.0 copy-done.2
  25.8 0.9 fusion.37
  26.7 0.0 copy-start
  26.7 0.8 copy-done
  27.5 1.0 broadcast_in_dim.38
  28.5 2.1 reshape.198
  30.6 5.7 %scatter_custom_fusion.1 = bf16[768,2048]{1,0:T(8,128)(2,1)S(1)} fusion(s32[512]{0:T(512)S(1)} %bitcast.57, bf16[512,2048]{1,0:T(8,128)(2,1)} %reshape.198, bf16[]{:T(256)} %constant.52.clone.1), kind=kCustom, calls=%fused_computation.31 | custom fusion | bytes 3146240 | tf_op jit(solution)/shard_map/scatter | solution.py:70
  36.2 2.8 %reshape.175 = bf16[128,6,2048]{2,1,0:T(8,128)(2,1)} reshape(bf16[768,2048]{1,0:T(8,128)(2,1)S(1)} %scatter_custom_fusion.1) | data formatting | bytes 6291456 | tf_op jit(solution)/shard_map/reshape | solution.py:74
  39.1 0.0 all-to-all-done
  39.1 10.2 %all-to-all-start.1 = ((bf16[128,6,2048]{2,1,0:T(8,128)(2,1)}), bf16[128,6,2048]{2,1,0:T(8,128)(2,1)}, u32[]{:S(2)}, u32[]{:S(2)}) async-start(bf16[128,6,2048]{2,1,0:T(8,128)(2,1)} %reshape.175), calls=%async_computation.1 | async-start | bytes 8388608 | tf_op jit(solution)/shard_map/all_to_all | solution.py:81
  49.3 0.2 all-gather.5.cloned.1.call-start
  49.5 0.5 all-gather.5.cloned.1.call-update
  50.1 0.1 copy.42
  50.1 54.9 %all-to-all-done.1 = bf16[128,6,2048]{2,1,0:T(8,128)(2,1)} async-done(((bf16[128,6,2048]{2,1,0:T(8,128)(2,1)}), bf16[128,6,2048]{2,1,0:T(8,128)(2,1)}, u32[]{:S(2)}, u32[]{:S(2)}) %all-to-all-start.1) | async-done | bytes 3145760 | tf_op jit(solution)/shard_map/all_to_all | solution.py:81
  105.0 0.0 copy-start.4
  105.0 6.7 %fusion.8 = f32[128,6,512]{2,0,1:T(8,128)S(1)} fusion(bf16[2,2048,512]{2,1,0:T(8,128)(2,1)} %param.14, bf16[128,6,2048]{2,1,0:T(8,128)(2,1)} %all-to-all-done.1), kind=kOutput, calls=%fused_computation.16 | convolution fusion | flops 1610612736 | bytes 7864320 | tf_op jit(solution)/shard_map/scd,df->scf/dot_general | solution.py:25
  111.7 0.0 copy-done.4
  111.7 6.9 %fusion.13 = f32[128,6,512]{2,0,1:T(8,128)} fusion(bf16[2,2048,512]{2,1,0:T(8,128)(2,1)S(1)} %copy-done.4, bf16[128,6,2048]{2,1,0:T(8,128)(2,1)} %all-to-all-done.1), kind=kOutput, calls=%fused_computation.21 | convolution fusion | flops 1610612736 | bytes 6815744 | tf_op jit(solution)/shard_map/scd,df->scf/dot_general | solution.py:25
  118.6 10.7 %convolution_convert_fusion = bf16[128,6,2048]{2,0,1:T(8,128)(2,1)} fusion(bf16[2,512,2048]{2,1,0:T(8,128)(2,1)} %param.16, f32[128,6,512]{2,0,1:T(8,128)S(1)} %fusion.8, bf16[2,2048,512]{2,1,0:T(8,128)(2,1)} %param.15, bf16[128,6,2048]{2,1,0:T(8,128)(2,1)} %all-to-all-done.1), kind=kOutput, calls=%fused_computation.4 | convolution fusion | flops 3225157632 | bytes 13107200 | tf_op jit(solution)/shard_map/scf,fd->scd/dot_general | solution.py:28
  129.3 8.9 %select_select_fusion = bf16[128,6,2048]{2,0,1:T(8,128)(2,1)S(1)} fusion(bf16[128,6,2048]{2,0,1:T(8,128)(2,1)} %convolution_convert_fusion, pred[128,6]{0,1:T(8,128)(4,1)S(1)} %get-tuple-element.6, pred[128,6]{0,1:T(8,128)(4,1)S(1)} %get-tuple-element.5, bf16[2,512,2048]{2,1,0:T(8,128)(2,1)} %param.16, f32[128,6,512]{2,0,1:T(8,128)} %fusion.13, ...), kind=kOutput, calls=%fused_computation.6 | convolution fusion | flops 3228303360 | bytes 16254464 | tf_op jit(solution)/shard_map/scf,fd->scd/dot_general | solution.py:28
  138.2 3.8 %copy.48 = bf16[128,6,2048]{2,1,0:T(8,128)(2,1)} copy(bf16[128,6,2048]{2,0,1:T(8,128)(2,1)S(1)} %select_select_fusion) | data formatting | bytes 6291456 | tf_op jit(solution)/shard_map/jit(_where)/select_n | solution.py:38
  142.1 0.0 copy-start.3
  142.1 5.4 %all-to-all-start.2 = ((bf16[128,6,2048]{2,1,0:T(8,128)(2,1)}), bf16[128,6,2048]{2,1,0:T(8,128)(2,1)}, u32[]{:S(2)}, u32[]{:S(2)}) async-start(bf16[128,6,2048]{2,1,0:T(8,128)(2,1)} %copy.48), calls=%async_computation.2 | async-start | bytes 8388608 | tf_op jit(solution)/shard_map/all_to_all | solution.py:85
  147.5 0.0 copy-done.3
  147.5 0.1 copy.49
  147.6 54.5 %all-to-all-done.2 = bf16[128,6,2048]{2,1,0:T(8,128)(2,1)} async-done(((bf16[128,6,2048]{2,1,0:T(8,128)(2,1)}), bf16[128,6,2048]{2,1,0:T(8,128)(2,1)}, u32[]{:S(2)}, u32[]{:S(2)}) %all-to-all-start.2) | async-done | bytes 3145760 | tf_op jit(solution)/shard_map/all_to_all | solution.py:85
  202.1 4.9 %reshape.176 = bf16[768,2048]{1,0:T(8,128)(2,1)S(1)} reshape(bf16[128,6,2048]{2,1,0:T(8,128)(2,1)} %all-to-all-done.2) | data formatting | bytes 6291456 | tf_op jit(solution)/shard_map/reshape | solution.py:86
  207.0 3.3 %gather_fusion = bf16[512,2048]{1,0:T(8,128)(2,1)} fusion(bf16[768,2048]{1,0:T(8,128)(2,1)S(1)} %reshape.176, s32[1024]{0:T(1024)S(1)} %pad_clamp_fusion), kind=kCustom, calls=%fused_computation | custom fusion | bytes 4196352 | tf_op jit(solution)/shard_map/gather | solution.py:87
  210.3 4.7 %reshape.177 = f32[128,4,2048]{2,1,0:T(4,128)} reshape(bf16[512,2048]{1,0:T(8,128)(2,1)} %gather_fusion) | data formatting | bytes 6291456 | tf_op jit(solution)/shard_map/convert_element_type | solution.py:88
  215.0 0.0 copy-start.1
  215.0 5.4 %multiply_reduce_fusion = f32[128,2048]{1,0:T(8,128)S(1)} fusion(f32[128,4,2048]{2,1,0:T(4,128)} %reshape.177, f32[128,4]{1,0:T(8,128)S(1)} %copy.49), kind=kLoop, calls=%fused_computation.3 | loop fusion | flops 1835008 | bytes 5244928 | tf_op jit(solution)/shard_map/reduce_sum | solution.py:88
  220.4 0.0 all-gather.3.cloned.1.call-done
  220.4 0.0 copy-done.1
  220.5 2.0 fusion.3
  222.5 0.0 all-gather.5.cloned.1.call-done
  222.5 4.2 %fusion = bf16[128,2048]{1,0:T(8,128)(2,1)} fusion(f32[128,2048]{1,0:T(8,128)S(1)} %multiply_reduce_fusion, bf16[512,2048]{0,1:T(8,128)(2,1)} %all-gather.5.cloned.1.call-done, bf16[128,2048]{1,0:T(8,128)(2,1)S(1)} %copy-done.1, bf16[2048,1024]{1,0:T(8,128)(2,1)} %all-gather.3.cloned.1.call-done, f32[128,512]{1,0:T(8,128)S(1)} %fusion.3), kind=kOutput, calls=%fused_computation.8 | convolution fusion | flops 537788416 | bytes 6553600 | tf_op jit(solution)/shard_map/dot_general | solution.py:93
  (13 shorter events, 0.2 us)
Async XLA Ops:
  6.5 19.2 %copy-start.2 = (bf16[128,2048]{1,0:T(8,128)(2,1)S(1)}, bf16[128,2048]{1,0:T(8,128)(2,1)}, u32[]{:S(2)}) copy-start(bf16[128,2048]{1,0:T(8,128)(2,1)} %param.10) | copy-start | bytes 1572868
  6.5 213.9 %all-gather.3.cloned.1.call-start = ((), (), s32[]{:S(2)}) async-start(), calls=%async_computation.3 | async-start | bytes 4227072 | tf_op jit(solution)/shard_map/all_gather | solution.py:11
  13.0 26.0 %all-to-all-start = ((s32[128,1,6]{2,1,0:T(1,128)}), s32[128,1,6]{2,1,0:T(1,128)S(1)}, u32[]{:S(2)}, u32[]{:S(2)}) async-start(s32[128,1,6]{2,1,0:T(1,128)} %bitcast.5), calls=%async_computation | async-start | bytes 131072 | tf_op jit(solution)/shard_map/all_to_all | solution.py:82
  26.7 0.8 copy-start
  39.1 65.9 %all-to-all-start.1 = ((bf16[128,6,2048]{2,1,0:T(8,128)(2,1)}), bf16[128,6,2048]{2,1,0:T(8,128)(2,1)}, u32[]{:S(2)}, u32[]{:S(2)}) async-start(bf16[128,6,2048]{2,1,0:T(8,128)(2,1)} %reshape.175), calls=%async_computation.1 | async-start | bytes 8388608 | tf_op jit(solution)/shard_map/all_to_all | solution.py:81
  49.3 173.2 %all-gather.5.cloned.1.call-start = ((), (), s32[]{:S(2)}) async-start(), calls=%async_computation.4 | async-start | bytes 2113536 | tf_op jit(solution)/shard_map/all_gather | solution.py:95
  105.0 6.7 %copy-start.4 = (bf16[2,2048,512]{2,1,0:T(8,128)(2,1)S(1)}, bf16[2,2048,512]{2,1,0:T(8,128)(2,1)}, u32[]{:S(2)}) copy-start(bf16[2,2048,512]{2,1,0:T(8,128)(2,1)} %param.14) | copy-start | bytes 12582916
  142.1 5.4 %copy-start.3 = (f32[128,4]{0,1:T(4,128)S(1)}, f32[128,4]{0,1:T(4,128)}, u32[]{:S(2)}) copy-start(f32[128,4]{0,1:T(4,128)} %param.13) | copy-start | bytes 6148
  142.1 60.0 %all-to-all-start.2 = ((bf16[128,6,2048]{2,1,0:T(8,128)(2,1)}), bf16[128,6,2048]{2,1,0:T(8,128)(2,1)}, u32[]{:S(2)}, u32[]{:S(2)}) async-start(bf16[128,6,2048]{2,1,0:T(8,128)(2,1)} %copy.48), calls=%async_computation.2 | async-start | bytes 8388608 | tf_op jit(solution)/shard_map/all_to_all | solution.py:85
  215.0 5.4 %copy-start.1 = (bf16[128,2048]{1,0:T(8,128)(2,1)S(1)}, bf16[128,2048]{1,0:T(8,128)(2,1)}, u32[]{:S(2)}) copy-start(bf16[128,2048]{1,0:T(8,128)(2,1)} %copy-done) | copy-start | bytes 1572868
Sparse Core Ops, SparseCore 0:
  10.5 101.0 all-gather.2
  114.7 89.0 all-gather.4
where the time goes:
time: 234 us
  waiting for transfers between devices  110 us (47%)
  matrix products  39.4 us (17%)
  local copies, waits for them, and re-layouts  33.7 us (14%)
  starting transfers between devices  27.3 us (12%)
  between operations  13.6 us (6%)
  other arithmetic  9.5 us (4%)
    all_to_all x1, waiting for transfers between devices, per_device(): lax.all_to_all(outgoing, 'ep', split_axis=0, concat_axis=0, tiled=True)  54.9 us
    all_to_all x1, waiting for transfers between devices, per_device(): lax.all_to_all(results, 'ep', split_axis=0, concat_axis=0, tiled=True)  54.5 us
    dot_general x2, matrix products, run_single(): jnp.einsum('scf,fd->scd', hidden, w_down, preferred_element_type=jnp.floa...  19.6 us
    dot_general x2, matrix products, run_single(): jnp.einsum('scd,df->scf', incoming, w_gate, preferred_element_type=jnp.fl...  13.6 us
    all_to_all x1, starting transfers between devices, per_device(): lax.all_to_all(labels, 'ep', split_axis=0, concat_axis=0, tiled=True)  11.5 us
    all_to_all x1, starting transfers between devices, per_device(): lax.all_to_all(outgoing, 'ep', split_axis=0, concat_axis=0, tiled=True)  10.2 us
    scatter x1, local copies, waits for them, and re-layouts, per_device(): jnp.zeros((devices_ep * capacity, width), jnp.bfloat16).at[position]  5.65 us
    all_to_all x1, starting transfers between devices, per_device(): lax.all_to_all(results, 'ep', split_axis=0, concat_axis=0, tiled=True)  5.41 us
  transfers between devices with their start and end apart: 5, of which 2 were waited for; matrix products, arithmetic and copies ran while one was open for 32% of the time, Pallas kernels for 0%

commit v1 on v0

v1 whole, which is shorter than its diff:
```python
import jax
import jax.numpy as jnp
from jax import lax
from jax.experimental import pallas as pl
from jax.experimental.pallas import tpu as pltpu
from jax.sharding import PartitionSpec as P

EPS = 1e-06
MESH = pl.DeviceIdType.MESH
F32, BF16 = jnp.float32, jnp.bfloat16

D = 2048
DE = 512
NJ = 4
F = D // NJ
LINE = 4
TOK = 128
CAP = 6
BLK = LINE * CAP
PEERS = 32
ROWS = PEERS * BLK
COLS = LINE * TOK
HS = 128
SLAB = 16

_CHIP = [(0, 1), (1, 0), (0, 3), (3, 0), (1, 1), (1, 3), (3, 1), (3, 3), (0, 2), (2, 0), (2, 1), (1, 2), (2, 3), (3, 2), (2, 2)]
PLANE = [(a, b, 0) for a, b in _CHIP] + [(0, 0, 1)] + [(a, b, 1) for a, b in _CHIP]
LINEK = (1, 3, 2)


def silu(v):
    return v / (1.0 + jnp.exp(-v))


def dot(a, b):
    return jnp.dot(a, b, preferred_element_type=F32)


def dot_t(a, b):
    return lax.dot_general(a, b, (((1,), (1,)), ((), ())), preferred_element_type=F32)


def row_pattern(shape, dim, offset):
    row = (lax.broadcasted_iota(jnp.int32, shape, dim) + offset).astype(F32)
    peer = jnp.floor((row + 0.5) * (1.0 / BLK))
    inner = row - BLK * peer
    line = jnp.floor((inner + 0.5) * (1.0 / CAP))
    slot = inner - CAP * line
    return peer, inner, 8.0 * line + slot + 1.0


def kernel(
    tok, gain, ids, gw, sg, su, sd, wg_hbm, wu_hbm, wd_hbm, out,
    wgu, wd, x4, meta, sown, sgather, wsg, wsu, wsd, vmat, bits, sel, wsel, lab_out, lab_in,
    send, got, gu, hid, back, ret, hs, part, parts,
    wsem, msem, ssem, xsem, lsem, dsem, rsem, psem,
):
    me = lax.axis_index("ep")
    z, y, x, c = lax.div(me, 32), lax.rem(lax.div(me, 8), 4), lax.rem(lax.div(me, 2), 4), lax.rem(me, 2)
    mine = lax.rem(me, 32)
    sends = []

    def remote(src, dst, landed, sems, at, dev, start=True):
        s, r = sems.at[(0,) + at], sems.at[(1,) + at]
        go = pltpu.make_async_remote_copy(src, dst, s, r, device_id=(dev,), device_id_type=MESH)
        go.start()
        sends.append(go)
        return pltpu.make_async_remote_copy(src, landed, s, r, device_id=(dev,), device_id_type=MESH)

    def on_z(k):
        return lax.rem(z + k, 4), lax.rem(z + 4 - k, 4)

    def zdev(zz):
        return zz * 32 + mine

    plane = []
    for dy, dx, dc in PLANE:
        to = lax.rem(y + dy, 4) * 8 + lax.rem(x + dx, 4) * 2 + lax.rem(c + dc, 2)
        frm = lax.rem(y + 4 - dy, 4) * 8 + lax.rem(x + 4 - dx, 4) * 2 + lax.rem(c + dc, 2)
        plane.append((to, frm, z * 32 + to))

    def rows_of(b):
        return pl.ds(pl.multiple_of(b * BLK, 8), BLK)

    def toks_of(zz):
        return pl.ds(pl.multiple_of(zz * TOK, TOK), TOK)

    barrier = pltpu.get_barrier_semaphore()
    for k in LINEK:
        pl.semaphore_signal(barrier, inc=1, device_id=(zdev(on_z(k)[0]),), device_id_type=MESH)
    for _, _, dev in plane:
        pl.semaphore_signal(barrier, inc=1, device_id=(dev,), device_id_type=MESH)

    weights = []
    for e in range(2):
        weights.append(pltpu.make_async_copy(wg_hbm.at[e], wgu.at[2 * e], wsem.at[3 * e]))
        weights.append(pltpu.make_async_copy(wu_hbm.at[e], wgu.at[2 * e + 1], wsem.at[3 * e + 1]))
    for e in range(2):
        weights.append(pltpu.make_async_copy(wd_hbm.at[e], wd.at[pl.ds(e * DE, DE)], wsem.at[3 * e + 2]))
    for w in weights:
        w.start()

    meta[z, 0:4, :] = ids[...].astype(F32)
    meta[z, 4:8, :] = gw[...]

    def norm_tile(i, carry):
        r = pl.ds(pl.multiple_of(i * 16, 16), 16)
        t = tok[r, :].astype(F32)
        t = t * lax.rsqrt(jnp.mean(t * t, axis=-1, keepdims=True) + EPS)
        t = (t * gain[...]).astype(BF16)
        at = pl.ds(pl.multiple_of(z * TOK + i * 16, 16), 16)
        for j in range(NJ):
            x4[j, at, :] = t[:, j * F:(j + 1) * F]
        return carry

    lax.fori_loop(0, TOK // 16, norm_tile, 0)
    for q in range(4):
        cut = slice(q * HS, (q + 1) * HS)
        sown[q, 0:SLAB, :] = sg[:, cut]
        sown[q, SLAB:2 * SLAB, :] = su[:, cut]
        sown[q, 2 * SLAB:3 * SLAB, :] = sd[:, cut]
    sgather[c, x, y, z] = sown[z]

    pl.semaphore_wait(barrier, len(LINEK) + len(PLANE))

    meta_in, slab_z, x_in = [], [], [[] for _ in range(NJ)]
    for k in LINEK:
        to, frm = on_z(k)
        meta_in.append(remote(meta.at[z], meta.at[z], meta.at[frm], msem, (k - 1,), zdev(to)))

    def send_x(j):
        for k in LINEK:
            to, frm = on_z(k)
            x_in[j].append(remote(x4.at[j, toks_of(z)], x4.at[j, toks_of(z)], x4.at[j, toks_of(frm)], xsem, (j, k - 1), zdev(to)))

    send_x(0)
    for k in LINEK:
        to, frm = on_z(k)
        slab_z.append(remote(sown.at[to], sgather.at[c, x, y, z], sgather.at[c, x, y, frm], ssem, (k - 1,), zdev(to)))
    for j in range(1, NJ):
        send_x(j)

    for m in meta_in:
        m.wait_recv()
    here = lax.broadcasted_iota(jnp.int32, (PEERS, TOK), 0).astype(F32) + (z * PEERS).astype(F32)
    before = (
        lax.broadcasted_iota(jnp.int32, (TOK, TOK), 0) < lax.broadcasted_iota(jnp.int32, (TOK, TOK), 1)
    ).astype(F32).astype(BF16)
    wvals, slots, whichs = [], [], []
    for q in range(LINE):
        hit = jnp.zeros((PEERS, TOK), F32)
        wv = jnp.zeros((PEERS, TOK), F32)
        bit = jnp.zeros((PEERS, TOK), F32)
        for k in range(4):
            e = meta[q, k:k + 1, :]
            dev = jnp.floor(e * 0.5)
            is_k = (here == dev).astype(F32)
            hit = hit + is_k
            wv = wv + is_k * meta[q, 4 + k:5 + k, :]
            bit = bit + is_k * (e - 2.0 * dev)
        rank = dot(hit.astype(BF16), before)
        slots.append(jnp.where(hit > 0.0, rank + (8.0 * q + 1.0), 0.0))
        wvals.append(wv)
        whichs.append(bit)
    lane = lax.broadcasted_iota(jnp.int32, (PEERS, 128), 1)
    labels = jnp.zeros((PEERS, 128), F32)
    for q in range(LINE):
        for s in range(CAP):
            bit = jnp.sum(jnp.where(slots[q] == 8.0 * q + s + 1.0, whichs[q], 0.0), axis=1, keepdims=True)
            labels = jnp.where(lane == q * CAP + s, bit, labels)
    for b in range(PEERS):
        lab_out[b] = labels[b:b + 1, :]
    lab_in[mine] = lab_out[mine]

    pad = jnp.zeros((128 - PEERS, TOK), F32)
    for q in range(LINE):
        cut = slice(q * TOK, (q + 1) * TOK)
        vmat[0, :, cut] = jnp.concatenate([slots[q], pad], axis=0).astype(BF16)
        bits[0, cut, :] = jnp.transpose(jnp.concatenate([slots[q], pad], axis=0)).astype(BF16)
        bits[1, cut, :] = jnp.transpose(jnp.concatenate([wvals[q], pad], axis=0)).astype(BF16)

    def sel_tile(i, carry):
        peer, _, target = row_pattern((128, 128), 0, i * 128)
        pick = (peer == lax.broadcasted_iota(jnp.int32, (128, 128), 1).astype(F32)).astype(F32).astype(BF16)
        val = dot(pick, vmat[0])
        sel[pl.ds(pl.multiple_of(i * 128, 128), 128), :] = (val == target[:, 0:1]).astype(F32).astype(BF16)
        return carry

    lax.fori_loop(0, ROWS // 128, sel_tile, 0)

    def dispatch(j):
        for n in range(F // 256):
            cut = slice(n * 256, (n + 1) * 256)
            send[j, :, cut] = dot(sel[...], x4[j, :, cut]).astype(BF16)
        arrivals = []
        for i, (to, frm, dev) in enumerate(plane):
            arrivals.append(remote(send.at[j, rows_of(to)], got.at[j, rows_of(mine)], got.at[j, rows_of(frm)], dsem, (j, i), dev))
        got[j, rows_of(mine), :] = send[j, rows_of(mine), :]
        return arrivals

    got_in = []
    for m in x_in[0]:
        m.wait_recv()
    got_in.append(dispatch(0))
    label_in = [
        remote(lab_out.at[to], lab_in.at[mine], lab_in.at[frm], lsem, (i,), dev)
        for i, (to, frm, dev) in enumerate(plane)
    ]
    for m in slab_z:
        m.wait_recv()
    slab_y = []
    for k in LINEK:
        to, frm = lax.rem(y + k, 4), lax.rem(y + 4 - k, 4)
        slab_y.append(remote(sgather.at[c, x, y], sgather.at[c, x, y], sgather.at[c, x, frm], ssem, (2 + k,), z * 32 + to * 8 + x * 2 + c))
    for m in x_in[1]:
        m.wait_recv()
    got_in.append(dispatch(1))
    for m in slab_y:
        m.wait_recv()
    slab_x = []
    for k in LINEK:
        to, frm = lax.rem(x + k, 4), lax.rem(x + 4 - k, 4)
        slab_x.append(remote(sgather.at[c, x], sgather.at[c, x], sgather.at[c, frm], ssem, (5 + k,), z * 32 + y * 8 + to * 2 + c))
    for j in range(2, NJ):
        for m in x_in[j]:
            m.wait_recv()
        got_in.append(dispatch(j))

    def wsel_tile(i, carry):
        peer, _, target = row_pattern((128, 128), 1, i * 128)
        pick = (peer == lax.broadcasted_iota(jnp.int32, (128, 128), 0).astype(F32)).astype(F32).astype(BF16)
        val = dot(bits[0], pick)
        w = dot(bits[1], pick)
        wsel[:, pl.ds(pl.multiple_of(i * 128, 128), 128)] = jnp.where(val == target[0:1, :], w, 0.0).astype(BF16)
        return carry

    lax.fori_loop(0, ROWS // 128, wsel_tile, 0)

    for m in slab_x:
        m.wait_recv()
    slab_c = remote(sgather.at[c], sgather.at[c], sgather.at[1 - c], ssem, (9,), z * 32 + y * 8 + x * 2 + 1 - c)

    for m in label_in:
        m.wait_recv()
    for w in weights:
        w.wait()

    vmat[1] = jnp.zeros((128, COLS), BF16)
    for b in range(PEERS):
        bits[2, b:b + 1, :] = lab_in[b].astype(BF16)

    for j in range(NJ - 1):
        for m in got_in[j]:
            m.wait_recv()

        def accumulate(n, carry, j=j):
            q = lax.div(n, 2)
            cut = pl.ds(pl.multiple_of(lax.rem(n, 2) * 256, 256), 256)
            prod = dot(got[j], wgu[q, j * F:(j + 1) * F, cut])
            if j == 0:
                gu[q, :, cut] = prod
            else:
                gu[q, :, cut] += prod
            return carry

        lax.fori_loop(0, 8, accumulate, 0)

    peer, inner, _ = row_pattern((ROWS, 128), 0, 0)
    lane = lax.broadcasted_iota(jnp.int32, (ROWS, 128), 1).astype(F32)
    pick = (peer == lane).astype(F32)
    lab = dot(pick.astype(BF16)[:, 0:PEERS], bits[2, 0:PEERS, :])
    which = jnp.sum(jnp.where(inner == lane, lab, 0.0), axis=1, keepdims=True)

    j = NJ - 1
    for m in got_in[j]:
        m.wait_recv()
    for e in range(2):
        keep = which if e == 1 else 1.0 - which
        for n in range(2):
            cut = slice(n * 256, (n + 1) * 256)
            g = gu[2 * e, :, cut] + dot(got[j], wgu[2 * e, j * F:(j + 1) * F, cut])
            u = gu[2 * e + 1, :, cut] + dot(got[j], wgu[2 * e + 1, j * F:(j + 1) * F, cut])
            hid[:, e * DE + n * 256:e * DE + (n + 1) * 256] = (silu(g) * u * keep).astype(BF16)

    ret_in = []
    for j in range(NJ):
        for n in range(F // 256):
            back[j, :, n * 256:(n + 1) * 256] = dot(hid[...], wd[:, j * F + n * 256:j * F + (n + 1) * 256]).astype(BF16)
        arrivals = []
        for i, (to, frm, dev) in enumerate(plane):
            arrivals.append(remote(back.at[j, rows_of(to)], ret.at[j, rows_of(mine)], ret.at[j, rows_of(frm)], rsem, (j, i), dev))
        ret[j, rows_of(mine), :] = back[j, rows_of(mine), :]
        ret_in.append(arrivals)

    slab_c.wait_recv()
    for zz in range(4):
        for yy in range(4):
            for xx in range(4):
                for cc in range(2):
                    r = (((zz * 4 + yy) * 4 + xx) * 2 + cc) * SLAB
                    wsg[r:r + SLAB, :] = sgather[cc, xx, yy, zz, 0:SLAB, :]
                    wsu[r:r + SLAB, :] = sgather[cc, xx, yy, zz, SLAB:2 * SLAB, :]
                    wsd[r:r + SLAB, :] = sgather[cc, xx, yy, zz, 2 * SLAB:3 * SLAB, :]
    g = jnp.zeros((COLS, HS), F32)
    u = jnp.zeros((COLS, HS), F32)
    for j in range(NJ):
        g = g + dot(x4[j], wsg[j * F:(j + 1) * F, :])
        u = u + dot(x4[j], wsu[j * F:(j + 1) * F, :])
    hs[...] = (silu(g) * u).astype(BF16)

    part_in = []
    for j in range(NJ):
        for m in ret_in[j]:
            m.wait_recv()
        for n in range(F // 256):
            at = j * F + n * 256
            val = dot(wsel[...], ret[j, :, n * 256:(n + 1) * 256]) + dot_t(hs[...], wsd[at:at + 256, :])
            part[j, :, n * 256:(n + 1) * 256] = val.astype(BF16)
        arrivals = []
        for k in LINEK:
            to, frm = on_z(k)
            arrivals.append(remote(part.at[j, toks_of(to)], parts.at[j, toks_of(z)], parts.at[j, toks_of(frm)], psem, (j, k - 1), zdev(to)))
        parts[j, toks_of(z), :] = part[j, toks_of(z), :]
        part_in.append(arrivals)

    for j in range(NJ):
        for m in part_in[j]:
            m.wait_recv()
        total = parts[j, 0:TOK, :].astype(F32)
        for q in range(1, LINE):
            total = total + parts[j, q * TOK:(q + 1) * TOK, :].astype(F32)
        out[:, j * F:(j + 1) * F] = total.astype(BF16)

    for s in sends:
        s.wait_send()


def per_device(tokens, norm_gain, expert_ids, gate_weights, expert_gate, expert_up, expert_down, shared_gate, shared_up, shared_down):
    vmem = pl.BlockSpec(memory_space=pltpu.VMEM)
    hbm = pl.BlockSpec(memory_space=pl.ANY)
    dma = pltpu.SemaphoreType.DMA
    n = len(PLANE)
    return pl.pallas_call(
        kernel,
        out_shape=jax.ShapeDtypeStruct((TOK, D), BF16),
        in_specs=[vmem] * 7 + [hbm] * 3,
        out_specs=vmem,
        scratch_shapes=[
            pltpu.VMEM((4, D, DE), BF16),
            pltpu.VMEM((2 * DE, D), BF16),
            pltpu.VMEM((NJ, COLS, F), BF16),
            pltpu.VMEM((LINE, 8, TOK), F32),
            pltpu.VMEM((4, 3 * SLAB, HS), BF16),
            pltpu.VMEM((2, 4, 4, 4, 3 * SLAB, HS), BF16),
            pltpu.VMEM((D, HS), BF16),
            pltpu.VMEM((D, HS), BF16),
            pltpu.VMEM((D, HS), BF16),
            pltpu.VMEM((2, 128, COLS), BF16),
            pltpu.VMEM((3, COLS, 128), BF16),
            pltpu.VMEM((ROWS, COLS), BF16),
            pltpu.VMEM((COLS, ROWS), BF16),
            pltpu.VMEM((PEERS, 1, 128), F32),
            pltpu.VMEM((PEERS, 1, 128), F32),
            pltpu.VMEM((NJ, ROWS, F), BF16),
            pltpu.VMEM((NJ, ROWS, F), BF16),
            pltpu.VMEM((4, ROWS, DE), F32),
            pltpu.VMEM((ROWS, 2 * DE), BF16),
            pltpu.VMEM((NJ, ROWS, F), BF16),
            pltpu.VMEM((NJ, ROWS, F), BF16),
            pltpu.VMEM((COLS, HS), BF16),
            pltpu.VMEM((NJ, COLS, F), BF16),
            pltpu.VMEM((NJ, COLS, F), BF16),
            dma((6,)),
            dma((2, 3)),
            dma((2, 10)),
            dma((2, NJ, 3)),
            dma((2, n)),
            dma((2, NJ, n)),
            dma((2, NJ, n)),
            dma((2, NJ, 3)),
        ],
        compiler_params=pltpu.CompilerParams(
            collective_id=0, has_side_effects=True, vmem_limit_bytes=67043328
        ),
        name="moe",
    )(
        tokens, norm_gain.reshape(1, D), expert_ids.T, gate_weights.T,
        shared_gate, shared_up, shared_down.T, expert_gate, expert_up, expert_down,
    )


def solution(mesh):
    ep = P("ep")
    return jax.shard_map(
        per_device,
        mesh=mesh,
        in_specs=(ep, P(), ep, ep, ep, ep, ep, ep, ep, P(None, "ep")),
        out_specs=ep,
        check_vma=False,
    )
```

time: 234 us -> 118 us (0.50)
  Pallas kernels: 0 us -> 116 us
  waiting for transfers between devices: 110 us -> 0 us
  matrix products: 39.4 us -> 0 us
  local copies, waits for them, and re-layouts: 33.7 us -> 1.88 us
  starting transfers between devices: 27.3 us -> 0 us
  between operations: 13.6 us -> 0.01 us
  other arithmetic: 9.5 us -> 0 us
    pallas_call x0 -> x1, Pallas kernels: none -> 116 us  [per_device(): pl.pallas_call(kernel, out_shape=jax.ShapeDtypeStruct((TOK, D), BF16), in...]
    all_to_all x3 -> x0, waiting for transfers between devices: 109 us -> none  [the longest x1 54.9 us: per_device(): lax.all_to_all(outgoing, 'ep', split_axis=0, concat_axis=0, tiled=True)]
    dot_general x6 -> x0, matrix products: 39.4 us -> none  [the longest x2 19.6 us: run_single(): jnp.einsum('scf,fd->scd', hidden, w_down, preferred_element_type=jnp.floa...]
    all_to_all x3 -> x0, starting transfers between devices: 27.1 us -> none  [the longest x1 11.5 us: per_device(): lax.all_to_all(labels, 'ep', split_axis=0, concat_axis=0, tiled=True)]
    reshape x6 -> x0, local copies, waits for them, and re-layouts: 10.1 us -> none  [the longest x1 4.87 us: per_device(): returned = returned.reshape(devices_ep * capacity, width)]
    scatter x2 -> x0, local copies, waits for them, and re-layouts: 8.1 us -> none  [the longest x1 5.65 us: per_device(): jnp.zeros((devices_ep * capacity, width), jnp.bfloat16).at[position]]
    reduce_sum x3 -> x0, other arithmetic: 6.86 us -> none  [the longest x1 5.4 us: per_device(): jnp.sum(picked.astype(jnp.float32) * gate_weights[:, :, None], axis=1)]
    convert_element_type x1 -> x0, local copies, waits for them, and re-layouts: 4.74 us -> none  [per_device(): picked.astype(jnp.float32) * gate_weights[:, :, None]]
  transfers between devices with their start and end apart: 5 -> 0, of which waited for: 2 -> 0; matrix products, arithmetic and copies ran while one was open for 32% -> 0% of each run, Pallas kernels for 0% -> 0%
where the time goes in v1:
time: 118 us
  Pallas kernels  116 us (98%)
  local copies, waits for them, and re-layouts  1.88 us (2%)
    pallas_call x1, Pallas kernels, per_device(): pl.pallas_call(kernel, out_shape=jax.ShapeDtypeStruct((TOK, D), BF16), in...  116 us

profile of v1, /device:TPU:1, one launch (start us, length us, event | category | flops | bytes accessed | tf_op | source)
XLA Modules:
  0.0 118.3 jit_solution(14085301537453503101)
XLA Ops:
  0.0 116.4 %moe.1 = bf16[128,2048]{1,0:T(8,128)(2,1)} custom-call(bf16[128,2048]{1,0:T(8,128)(2,1)} %tok.1, f32[1,2048]{1,0:T(1,128)} %bitcast.5, s32[4,128]{1,0:T(4,128)} %bitcast.6, f32[4,128]{1,0:T(4,128)} %bitcast.7, bf16[16,512]{1,0:T(8,128)(2,1)} %sg.1, bf16[16,512]{1,0:T(8,128)(2,1)} %su.1, bf16[16,512]{1,0:T(8,128)(2,1)} %bitcast.4, ...), custom_call_target="tpu_custom_call" | custom-call | tf_op jit(solution)/shard_map/moe/pallas_call | solution.py:343
  116.4 1.9 %copy.12 = bf16[128,2048]{1,0:T(8,128)(2,1)} copy(bf16[128,2048]{1,0:T(8,128)(2,1)} %moe.1) | data formatting | bytes 1048576

commit v2 on v1

v2 whole, which is shorter than its diff:
```python
import jax
import jax.numpy as jnp
from jax import lax
from jax.experimental import pallas as pl
from jax.experimental.pallas import tpu as pltpu
from jax.sharding import PartitionSpec as P

EPS = 1e-06
MESH = pl.DeviceIdType.MESH
F32, BF16 = jnp.float32, jnp.bfloat16

D = 2048
DE = 512
F = 256
NS = D // F
GROUPS = [(0, 1), (1, 3), (3, 5), (5, 7), (7, 8)]
NG = len(GROUPS)
LINE = 4
TOK = 128
CAP = 6
BLK = LINE * CAP
PEERS = 32
ROWS = PEERS * BLK
COLS = LINE * TOK
HS = 128
SLAB = 16

_CHIP = [(0, 1), (1, 0), (0, 3), (3, 0), (1, 1), (1, 3), (3, 1), (3, 3), (0, 2), (2, 0), (2, 1), (1, 2), (2, 3), (3, 2), (2, 2)]
PLANE = [(a, b, 0) for a, b in _CHIP] + [(0, 0, 1)] + [(a, b, 1) for a, b in _CHIP]
LINEK = (1, 3, 2)


def silu(v):
    return v / (1.0 + jnp.exp(-v))


def dot(a, b):
    return jnp.dot(a, b, preferred_element_type=F32)


def dot_t(a, b):
    return lax.dot_general(a, b, (((1,), (1,)), ((), ())), preferred_element_type=F32)


def row_pattern(shape, dim, offset):
    row = (lax.broadcasted_iota(jnp.int32, shape, dim) + offset).astype(F32)
    peer = jnp.floor((row + 0.5) * (1.0 / BLK))
    inner = row - BLK * peer
    line = jnp.floor((inner + 0.5) * (1.0 / CAP))
    slot = inner - CAP * line
    return peer, inner, 8.0 * line + slot + 1.0


def kernel(
    tok_hbm, gain_hbm, ids_hbm, gw_hbm, sg_hbm, su_hbm, sd_hbm, wg_hbm, wu_hbm, wd_hbm, out_hbm,
    tok, gain, ids, gw, sg, su, sd,
    wgu, wd, x4, meta, sown, sgather, wsg, wsu, wsd, vmat, bits, sel, wsel, lab_out, lab_in,
    send, got, gu, hid, back, ret, hs, part, parts, out,
    isem, wsem, osem, msem, ssem, xsem, lsem, dsem, rsem, psem,
):
    me = lax.axis_index("ep")
    z, y, x, c = lax.div(me, 32), lax.rem(lax.div(me, 8), 4), lax.rem(lax.div(me, 2), 4), lax.rem(me, 2)
    mine = lax.rem(me, 32)
    sends = []

    def copy_to(src, dst, sems, at, dev):
        return pltpu.make_async_remote_copy(src, dst, sems.at[(0,) + at], sems.at[(1,) + at], device_id=(dev,), device_id_type=MESH)

    def remote(src, dst, landed, sems, at, dev):
        go = copy_to(src, dst, sems, at, dev)
        go.start()
        sends.append(go)
        return copy_to(src, landed, sems, at, dev)

    def line(v, k):
        return lax.rem(v + k, 4), lax.rem(v + 4 - k, 4)

    def zdev(zz):
        return zz * 32 + mine

    def pdev(yy, xx, cc):
        return z * 32 + yy * 8 + xx * 2 + cc

    plane = []
    for dy, dx, dc in PLANE:
        to = lax.rem(y + dy, 4) * 8 + lax.rem(x + dx, 4) * 2 + lax.rem(c + dc, 2)
        plane.append((to, z * 32 + to))

    def rows_of(b):
        return pl.ds(pl.multiple_of(b * BLK, 8), BLK)

    def toks_of(zz):
        return pl.ds(pl.multiple_of(zz * TOK, TOK), TOK)

    def exchange(src, dst, group, sems):
        a, b = GROUPS[group]
        for to, dev in plane:
            copy_to(src.at[a:b, rows_of(to)], dst.at[a:b, rows_of(mine)], sems, (group,), dev).start()
        for q in range(a, b):
            dst[q, rows_of(mine), :] = src[q, rows_of(mine), :]
        every = pl.ds(0, len(plane) * BLK)
        done = copy_to(src.at[a:b, every], dst.at[a:b, every], sems, (group,), plane[0][1])
        sends.append(done)
        return done

    small = [
        pltpu.make_async_copy(src, dst, isem.at[i])
        for i, (src, dst) in enumerate(
            [(tok_hbm, tok), (gain_hbm, gain), (ids_hbm, ids), (gw_hbm, gw), (sg_hbm, sg), (su_hbm, su), (sd_hbm, sd)]
        )
    ]
    for m in small:
        m.start()

    barrier = pltpu.get_barrier_semaphore()
    for k in LINEK:
        pl.semaphore_signal(barrier, inc=1, device_id=(zdev(line(z, k)[0]),), device_id_type=MESH)
    for _, dev in plane:
        pl.semaphore_signal(barrier, inc=1, device_id=(dev,), device_id_type=MESH)

    weights = []
    for e in range(2):
        weights.append(pltpu.make_async_copy(wg_hbm.at[e], wgu.at[2 * e], wsem.at[3 * e]))
        weights.append(pltpu.make_async_copy(wu_hbm.at[e], wgu.at[2 * e + 1], wsem.at[3 * e + 1]))
    for e in range(2):
        weights.append(pltpu.make_async_copy(wd_hbm.at[e], wd.at[pl.ds(e * DE, DE)], wsem.at[3 * e + 2]))
    for m in small:
        m.wait()
    for w in weights:
        w.start()

    meta[z, 0:4, :] = ids[...].astype(F32)
    meta[z, 4:8, :] = gw[...]
    for q in range(4):
        cut = slice(q * HS, (q + 1) * HS)
        sown[q, 0:SLAB, :] = sg[:, cut]
        sown[q, SLAB:2 * SLAB, :] = su[:, cut]
        sown[q, 2 * SLAB:3 * SLAB, :] = sd[:, cut]
    sgather[c, x, y, z] = sown[z]

    def norm_tile(i, carry):
        r = pl.ds(pl.multiple_of(i * 16, 16), 16)
        t = tok[r, :].astype(F32)
        t = t * lax.rsqrt(jnp.mean(t * t, axis=-1, keepdims=True) + EPS)
        t = (t * gain[...]).astype(BF16)
        at = pl.ds(pl.multiple_of(z * TOK + i * 16, 16), 16)
        for q in range(NS):
            x4[q, at, :] = t[:, q * F:(q + 1) * F]
        return carry

    lax.fori_loop(0, TOK // 16, norm_tile, 0)

    pl.semaphore_wait(barrier, len(LINEK) + len(PLANE))

    meta_in, slab_z, x_in = [], [], [[] for _ in range(NG)]
    for k in LINEK:
        to, frm = line(z, k)
        slab_z.append(remote(sown.at[to], sgather.at[c, x, y, z], sgather.at[c, x, y, frm], ssem, (k - 1,), zdev(to)))
    for k in LINEK:
        to, frm = line(z, k)
        meta_in.append(remote(meta.at[z], meta.at[z], meta.at[frm], msem, (k - 1,), zdev(to)))
    for g, (a, b) in enumerate(GROUPS):
        for k in LINEK:
            to, frm = line(z, k)
            x_in[g].append(remote(x4.at[a:b, toks_of(z)], x4.at[a:b, toks_of(z)], x4.at[a:b, toks_of(frm)], xsem, (g, k - 1), zdev(to)))

    half = 3 * SLAB // 2
    top, low = pl.ds(0, half), pl.ds(half, half)
    for m in slab_z:
        m.wait_recv()
    slab_1, slab_2 = [], []
    for k in LINEK:
        to, frm = line(y, k)
        slab_1.append(remote(sgather.at[c, x, y, :, top], sgather.at[c, x, y, :, top], sgather.at[c, x, frm, :, top], ssem, (2 + k,), pdev(to, x, c)))
        to, frm = line(x, k)
        slab_1.append(remote(sgather.at[c, x, y, :, low], sgather.at[c, x, y, :, low], sgather.at[c, frm, y, :, low], ssem, (5 + k,), pdev(y, to, c)))

    for m in meta_in:
        m.wait_recv()
    here = lax.broadcasted_iota(jnp.int32, (PEERS, TOK), 0).astype(F32) + (z * PEERS).astype(F32)
    before = (
        lax.broadcasted_iota(jnp.int32, (TOK, TOK), 0) < lax.broadcasted_iota(jnp.int32, (TOK, TOK), 1)
    ).astype(F32).astype(BF16)
    wvals, slots, whichs = [], [], []
    for q in range(LINE):
        hit = jnp.zeros((PEERS, TOK), F32)
        wv = jnp.zeros((PEERS, TOK), F32)
        bit = jnp.zeros((PEERS, TOK), F32)
        for k in range(4):
            e = meta[q, k:k + 1, :]
            dev = jnp.floor(e * 0.5)
            is_k = (here == dev).astype(F32)
            hit = hit + is_k
            wv = wv + is_k * meta[q, 4 + k:5 + k, :]
            bit = bit + is_k * (e - 2.0 * dev)
        rank = dot(hit.astype(BF16), before)
        slots.append(jnp.where(hit > 0.0, rank + (8.0 * q + 1.0), 0.0))
        wvals.append(wv)
        whichs.append(bit)

    pad = jnp.zeros((128 - PEERS, TOK), F32)
    for q in range(LINE):
        cut = slice(q * TOK, (q + 1) * TOK)
        vmat[:, cut] = jnp.concatenate([slots[q], pad], axis=0).astype(BF16)

    def sel_tile(i, carry):
        peer, _, target = row_pattern((128, 128), 0, i * 128)
        pick = (peer == lax.broadcasted_iota(jnp.int32, (128, 128), 1).astype(F32)).astype(F32).astype(BF16)
        val = dot(pick, vmat[...])
        sel[pl.ds(pl.multiple_of(i * 128, 128), 128), :] = (val == target[:, 0:1]).astype(F32).astype(BF16)
        return carry

    lax.fori_loop(0, ROWS // 128, sel_tile, 0)

    for m in slab_1:
        m.wait_recv()
    for k in LINEK:
        to, frm = line(x, k)
        slab_2.append(remote(sgather.at[c, x, :, :, top], sgather.at[c, x, :, :, top], sgather.at[c, frm, :, :, top], ssem, (8 + k,), pdev(y, to, c)))
        to, frm = line(y, k)
        slab_2.append(remote(sgather.at[c, :, y, :, low], sgather.at[c, :, y, :, low], sgather.at[c, :, frm, :, low], ssem, (11 + k,), pdev(to, x, c)))

    def dispatch(g):
        for m in x_in[g]:
            m.wait_recv()
        for q in range(*GROUPS[g]):
            send[q] = dot(sel[...], x4[q]).astype(BF16)
        return exchange(send, got, g, dsem)

    got_in = [dispatch(0)]

    lane = lax.broadcasted_iota(jnp.int32, (PEERS, 128), 1)
    labels = jnp.zeros((PEERS, 128), F32)
    for q in range(LINE):
        for s in range(CAP):
            bit = jnp.sum(jnp.where(slots[q] == 8.0 * q + s + 1.0, whichs[q], 0.0), axis=1, keepdims=True)
            labels = jnp.where(lane == q * CAP + s, bit, labels)
    for b in range(PEERS):
        lab_out[b] = labels[b:b + 1, :]
    lab_in[mine] = lab_out[mine]
    for to, dev in plane:
        copy_to(lab_out.at[to], lab_in.at[mine], lsem, (), dev).start()
    every = pl.ds(0, len(plane))
    label_in = copy_to(lab_out.at[every], lab_in.at[every], lsem, (), plane[0][1])
    sends.append(label_in)
    for q in range(LINE):
        cut = slice(q * TOK, (q + 1) * TOK)
        bits[0, cut, :] = jnp.transpose(jnp.concatenate([slots[q], pad], axis=0)).astype(BF16)
        bits[1, cut, :] = jnp.transpose(jnp.concatenate([wvals[q], pad], axis=0)).astype(BF16)

    got_in.append(dispatch(1))
    for m in slab_2:
        m.wait_recv()
    slab_c = remote(sgather.at[c], sgather.at[c], sgather.at[1 - c], ssem, (15,), pdev(y, x, 1 - c))
    for g in range(2, NG):
        got_in.append(dispatch(g))

    def wsel_tile(i, carry):
        peer, _, target = row_pattern((128, 128), 1, i * 128)
        pick = (peer == lax.broadcasted_iota(jnp.int32, (128, 128), 0).astype(F32)).astype(F32).astype(BF16)
        val = dot(bits[0], pick)
        w = dot(bits[1], pick)
        wsel[:, pl.ds(pl.multiple_of(i * 128, 128), 128)] = jnp.where(val == target[0:1, :], w, 0.0).astype(BF16)
        return carry

    lax.fori_loop(0, ROWS // 128, wsel_tile, 0)

    for w in weights:
        w.wait()
    label_in.wait_recv()
    for b in range(PEERS):
        bits[2, b:b + 1, :] = lab_in[b].astype(BF16)
    peer, inner, _ = row_pattern((ROWS, 128), 0, 0)
    lane = lax.broadcasted_iota(jnp.int32, (ROWS, 128), 1).astype(F32)
    pick = (peer == lane).astype(F32)
    lab = dot(pick.astype(BF16)[:, 0:PEERS], bits[2, 0:PEERS, :])
    which = jnp.sum(jnp.where(inner == lane, lab, 0.0), axis=1, keepdims=True)

    def partial(group, q, cut):
        return sum(dot(got[s], wgu[q, s * F:(s + 1) * F, cut]) for s in range(*GROUPS[group]))

    for g in range(NG - 1):
        got_in[g].wait_recv()

        def accumulate(n, carry, g=g):
            q = lax.div(n, 2)
            cut = pl.ds(pl.multiple_of(lax.rem(n, 2) * 256, 256), 256)
            prod = partial(g, q, cut)
            if g == 0:
                gu[q, :, cut] = prod
            else:
                gu[q, :, cut] += prod
            return carry

        lax.fori_loop(0, 8, accumulate, 0)

    got_in[NG - 1].wait_recv()
    for e in range(2):
        keep = which if e == 1 else 1.0 - which
        for n in range(2):
            cut = slice(n * 256, (n + 1) * 256)
            g = gu[2 * e, :, cut] + partial(NG - 1, 2 * e, cut)
            u = gu[2 * e + 1, :, cut] + partial(NG - 1, 2 * e + 1, cut)
            hid[:, e * DE + n * 256:e * DE + (n + 1) * 256] = (silu(g) * u * keep).astype(BF16)

    ret_in = []
    for g in range(NG):
        for q in range(*GROUPS[g]):
            back[q] = dot(hid[...], wd[:, q * F:(q + 1) * F]).astype(BF16)
        ret_in.append(exchange(back, ret, g, rsem))

    slab_c.wait_recv()
    for zz in range(4):
        for yy in range(4):
            for xx in range(4):
                for cc in range(2):
                    r = (((zz * 4 + yy) * 4 + xx) * 2 + cc) * SLAB
                    wsg[r:r + SLAB, :] = sgather[cc, xx, yy, zz, 0:SLAB, :]
                    wsu[r:r + SLAB, :] = sgather[cc, xx, yy, zz, SLAB:2 * SLAB, :]
                    wsd[r:r + SLAB, :] = sgather[cc, xx, yy, zz, 2 * SLAB:3 * SLAB, :]
    g = jnp.zeros((COLS, HS), F32)
    u = jnp.zeros((COLS, HS), F32)
    for q in range(NS):
        g = g + dot(x4[q], wsg[q * F:(q + 1) * F, :])
        u = u + dot(x4[q], wsu[q * F:(q + 1) * F, :])
    hs[...] = (silu(g) * u).astype(BF16)

    part_in = []
    for g, (a, b) in enumerate(GROUPS):
        ret_in[g].wait_recv()
        for q in range(a, b):
            part[q] = (dot(wsel[...], ret[q]) + dot_t(hs[...], wsd[q * F:(q + 1) * F, :])).astype(BF16)
        arrivals = []
        for k in LINEK:
            to, frm = line(z, k)
            arrivals.append(remote(part.at[a:b, toks_of(to)], parts.at[a:b, toks_of(z)], parts.at[a:b, toks_of(frm)], psem, (g, k - 1), zdev(to)))
        for q in range(a, b):
            parts[q, toks_of(z), :] = part[q, toks_of(z), :]
        part_in.append(arrivals)

    stores = []
    for g, (a, b) in enumerate(GROUPS):
        for m in part_in[g]:
            m.wait_recv()
        for q in range(a, b):
            total = parts[q, 0:TOK, :].astype(F32)
            for k in range(1, LINE):
                total = total + parts[q, k * TOK:(k + 1) * TOK, :].astype(F32)
            out[:, q * F:(q + 1) * F] = total.astype(BF16)
        stores.append(pltpu.make_async_copy(out.at[:, a * F:b * F], out_hbm.at[:, a * F:b * F], osem.at[g]))
        stores[-1].start()

    for s in sends:
        s.wait_send()
    for s in stores:
        s.wait()


def per_device(tokens, norm_gain, expert_ids, gate_weights, expert_gate, expert_up, expert_down, shared_gate, shared_up, shared_down):
    hbm = pl.BlockSpec(memory_space=pl.ANY)
    dma = pltpu.SemaphoreType.DMA
    return pl.pallas_call(
        kernel,
        out_shape=jax.ShapeDtypeStruct((TOK, D), BF16),
        in_specs=[hbm] * 10,
        out_specs=hbm,
        scratch_shapes=[
            pltpu.VMEM((TOK, D), BF16),
            pltpu.VMEM((1, D), F32),
            pltpu.VMEM((4, TOK), jnp.int32),
            pltpu.VMEM((4, TOK), F32),
            pltpu.VMEM((SLAB, 4 * HS), BF16),
            pltpu.VMEM((SLAB, 4 * HS), BF16),
            pltpu.VMEM((SLAB, 4 * HS), BF16),
            pltpu.VMEM((4, D, DE), BF16),
            pltpu.VMEM((2 * DE, D), BF16),
            pltpu.VMEM((NS, COLS, F), BF16),
            pltpu.VMEM((LINE, 8, TOK), F32),
            pltpu.VMEM((4, 3 * SLAB, HS), BF16),
            pltpu.VMEM((2, 4, 4, 4, 3 * SLAB, HS), BF16),
            pltpu.VMEM((D, HS), BF16),
            pltpu.VMEM((D, HS), BF16),
            pltpu.VMEM((D, HS), BF16),
            pltpu.VMEM((128, COLS), BF16),
            pltpu.VMEM((3, COLS, 128), BF16),
            pltpu.VMEM((ROWS, COLS), BF16),
            pltpu.VMEM((COLS, ROWS), BF16),
            pltpu.VMEM((PEERS, 1, 128), F32),
            pltpu.VMEM((PEERS, 1, 128), F32),
            pltpu.VMEM((NS, ROWS, F), BF16),
            pltpu.VMEM((NS, ROWS, F), BF16),
            pltpu.VMEM((4, ROWS, DE), F32),
            pltpu.VMEM((ROWS, 2 * DE), BF16),
            pltpu.VMEM((NS, ROWS, F), BF16),
            pltpu.VMEM((NS, ROWS, F), BF16),
            pltpu.VMEM((COLS, HS), BF16),
            pltpu.VMEM((NS, COLS, F), BF16),
            pltpu.VMEM((NS, COLS, F), BF16),
            pltpu.VMEM((TOK, D), BF16),
            dma((7,)),
            dma((6,)),
            dma((NG,)),
            dma((2, 3)),
            dma((2, 16)),
            dma((2, NG, 3)),
            dma((2,)),
            dma((2, NG)),
            dma((2, NG)),
            dma((2, NG, 3)),
        ],
        compiler_params=pltpu.CompilerParams(
            collective_id=0, has_side_effects=True, vmem_limit_bytes=67043328
        ),
        name="moe",
    )(
        tokens, norm_gain.reshape(1, D), expert_ids.T, gate_weights.T,
        shared_gate, shared_up, shared_down.T, expert_gate, expert_up, expert_down,
    )


def solution(mesh):
    ep = P("ep")
    return jax.shard_map(
        per_device,
        mesh=mesh,
        in_specs=(ep, P(), ep, ep, ep, ep, ep, ep, ep, P(None, "ep")),
        out_specs=ep,
        check_vma=False,
    )
```

time: 118 us -> 105 us (0.89)
  Pallas kernels: 116 us -> 102 us
    pallas_call x1, Pallas kernels: 116 us -> 102 us  [per_device(): pl.pallas_call(kernel, out_shape=jax.ShapeDtypeStruct((TOK, D), BF16), in...]
where the time goes in v2:
time: 105 us; the launch traced here: 104 us
  Pallas kernels  102 us (97%)
  local copies, waits for them, and re-layouts  1.88 us (2%)
    pallas_call x1, Pallas kernels, per_device(): pl.pallas_call(kernel, out_shape=jax.ShapeDtypeStruct((TOK, D), BF16), in...  102 us

profile of v2, /device:TPU:1, one launch (start us, length us, event | category | flops | bytes accessed | tf_op | source)
XLA Modules:
  0.0 104.3 jit_solution(5266213185046992383)
XLA Ops:
  0.0 102.4 %moe.1 = bf16[128,2048]{1,0:T(8,128)(2,1)} custom-call(bf16[128,2048]{1,0:T(8,128)(2,1)} %tok_hbm.1, f32[1,2048]{1,0:T(1,128)} %bitcast.5, s32[4,128]{1,0:T(4,128)} %bitcast.6, f32[4,128]{1,0:T(4,128)} %bitcast.7, bf16[16,512]{1,0:T(8,128)(2,1)} %sg_hbm.1, bf16[16,512]{1,0:T(8,128)(2,1)} %su_hbm.1, bf16[16,512]{1,0:T(8,128)(2,1)} %bitcast.4, ...), custom_call_target="tpu_custom_call" | custom-call | tf_op jit(solution)/shard_map/moe/pallas_call | solution.py:362
  102.4 1.9 %copy.12 = bf16[128,2048]{1,0:T(8,128)(2,1)} copy(bf16[128,2048]{1,0:T(8,128)(2,1)} %moe.1) | data formatting | bytes 1048576

commit v3 on v2

v3 whole, which is shorter than its diff:
```python
import jax
import jax.numpy as jnp
from jax import lax
from jax.experimental import pallas as pl
from jax.experimental.pallas import tpu as pltpu
from jax.sharding import PartitionSpec as P

EPS = 1e-06
MESH = pl.DeviceIdType.MESH
F32, BF16 = jnp.float32, jnp.bfloat16

D = 2048
DE = 512
SIZES = [256, 512, 512, 512, 256]
NG = len(SIZES)
SETS = [[0, 1], [2, 3], [4]]
SPANS = [slice(sum(SIZES[:g]), sum(SIZES[:g + 1])) for g in range(NG)]
LINE = 4
TOK = 128
CAP = 6
BLK = LINE * CAP
PEERS = 32
ROWS = PEERS * BLK
HALF = ROWS // 2
COLS = LINE * TOK
HS = 128
SLAB = 16

_CHIP = [(0, 1), (1, 0), (0, 3), (3, 0), (1, 1), (1, 3), (3, 1), (3, 3), (0, 2), (2, 0), (2, 1), (1, 2), (2, 3), (3, 2), (2, 2)]
PLANE = [[(a, b, 0) for a, b in _CHIP], [(0, 0, 1)] + [(a, b, 1) for a, b in _CHIP]]
EARLY = 1
HEAD = 3
LINEK = (1, 3, 2)


def silu(v):
    return (0.5 * v) * (1.0 + jnp.tanh(0.5 * v))


def dot(a, b):
    return jnp.dot(a, b, preferred_element_type=F32)


def dot_t(a, b):
    return lax.dot_general(a, b, (((1,), (1,)), ((), ())), preferred_element_type=F32)


def row_pattern(shape, dim, offset):
    row = (lax.broadcasted_iota(jnp.int32, shape, dim) + offset).astype(F32)
    peer = jnp.floor((row + 0.5) * (1.0 / BLK))
    inner = row - BLK * peer
    line = jnp.floor((inner + 0.5) * (1.0 / CAP))
    slot = inner - CAP * line
    return peer, inner, 8.0 * line + slot + 1.0


def kernel(
    tok_hbm, gain_hbm, ids_hbm, gw_hbm, sg_hbm, su_hbm, sd_hbm, wg_hbm, wu_hbm, wd_hbm, out_hbm,
    tok, gain, ids, gw, sg, su, sd,
    wgu, wd, x4, meta, sown, sgather, wsg, wsu, wsd, vmat, bits, sel, wsel, lab_out, lab_in,
    send, got, gu, hid, back, ret, hs, part, parts, out,
    isem, wsem, osem, msem, ssem, xsem, lsem, dsem, rsem, psem,
):
    me = lax.axis_index("ep")
    z, y, x, c = lax.div(me, 32), lax.rem(lax.div(me, 8), 4), lax.rem(lax.div(me, 2), 4), lax.rem(me, 2)
    mine = lax.rem(me, 32)
    sends = []

    def copy_to(src, dst, sems, at, dev):
        return pltpu.make_async_remote_copy(src, dst, sems.at[(0,) + at], sems.at[(1,) + at], device_id=(dev,), device_id_type=MESH)

    def remote(src, dst, landed, sems, at, dev):
        go = copy_to(src, dst, sems, at, dev)
        go.start()
        sends.append(go)
        return copy_to(src, landed, sems, at, dev)

    def line(v, k):
        return lax.rem(v + k, 4), lax.rem(v + 4 - k, 4)

    def zdev(zz):
        return zz * 32 + mine

    def pdev(yy, xx, cc):
        return z * 32 + yy * 8 + xx * 2 + cc

    spot = y * 4 + x
    plane = []
    for h in range(2):
        plane.append([])
        for dy, dx, dc in PLANE[h]:
            chip = lax.rem(y + dy, 4) * 4 + lax.rem(x + dx, 4)
            plane[h].append((h * 16 + chip, z * 32 + chip * 2 + lax.rem(c + dc, 2)))
    everyone = plane[0] + plane[1]

    def rows_of(b):
        return pl.ds(pl.multiple_of(b * BLK, 8), BLK)

    def toks_of(zz):
        return pl.ds(pl.multiple_of(zz * TOK, TOK), TOK)

    def exchange(src, dst, group, h, sems):
        src, dst = src[group], dst[group]
        for to, dev in plane[h]:
            copy_to(src.at[rows_of(to)], dst.at[rows_of(h * 16 + spot)], sems, (group, h), dev).start()
        if h == 0:
            dst[rows_of(spot), :] = src[rows_of(spot), :]
        every = pl.ds(0, len(plane[h]) * BLK)
        done = copy_to(src.at[every], dst.at[every], sems, (group, h), plane[h][0][1])
        sends.append(done)
        return done

    small = [
        pltpu.make_async_copy(src, dst, isem.at[i])
        for i, (src, dst) in enumerate(
            [(tok_hbm, tok), (gain_hbm, gain), (ids_hbm, ids), (gw_hbm, gw), (sg_hbm, sg), (su_hbm, su), (sd_hbm, sd)]
        )
    ]
    for m in small:
        m.start()

    barrier = pltpu.get_barrier_semaphore()
    for k in LINEK:
        pl.semaphore_signal(barrier, inc=1, device_id=(zdev(line(z, k)[0]),), device_id_type=MESH)
    for _, dev in everyone:
        pl.semaphore_signal(barrier, inc=1, device_id=(dev,), device_id_type=MESH)

    weights = []
    for e in range(2):
        weights.append(pltpu.make_async_copy(wg_hbm.at[e], wgu.at[2 * e], wsem.at[3 * e]))
        weights.append(pltpu.make_async_copy(wu_hbm.at[e], wgu.at[2 * e + 1], wsem.at[3 * e + 1]))
    for e in range(2):
        weights.append(pltpu.make_async_copy(wd_hbm.at[e], wd.at[pl.ds(e * DE, DE)], wsem.at[3 * e + 2]))
    for m in small:
        m.wait()
    for w in weights:
        w.start()

    meta[z, 0:4, :] = ids[...].astype(F32)
    meta[z, 4:8, :] = gw[...]
    for q in range(4):
        cut = slice(q * HS, (q + 1) * HS)
        sown[x, y, q, 0:SLAB, :] = sg[:, cut]
        sown[x, y, q, SLAB:2 * SLAB, :] = su[:, cut]
        sown[x, y, q, 2 * SLAB:3 * SLAB, :] = sd[:, cut]

    def norm_tile(i, carry):
        r = pl.ds(pl.multiple_of(i * 16, 16), 16)
        t = tok[r, :].astype(F32)
        t = t * lax.rsqrt(jnp.mean(t * t, axis=-1, keepdims=True) + EPS)
        t = (t * gain[...]).astype(BF16)
        at = pl.ds(pl.multiple_of(z * TOK + i * 16, 16), 16)
        for g in range(NG):
            x4[g][at, :] = t[:, SPANS[g]]
        return carry

    lax.fori_loop(0, TOK // 16, norm_tile, 0)

    pl.semaphore_wait(barrier, len(LINEK) + len(everyone))

    meta_in, slab_1, slab_2, slab_z, x_in = [], [], [], [], [[] for _ in range(NG)]
    half = 3 * SLAB // 2
    top, low = pl.ds(0, half), pl.ds(half, half)
    for k in LINEK:
        to, frm = line(y, k)
        slab_1.append(remote(sown.at[x, y, :, top], sown.at[x, y, :, top], sown.at[x, frm, :, top], ssem, (k - 1,), pdev(to, x, c)))
        to, frm = line(x, k)
        slab_1.append(remote(sown.at[x, y, :, low], sown.at[x, y, :, low], sown.at[frm, y, :, low], ssem, (2 + k,), pdev(y, to, c)))
    for k in LINEK:
        to, frm = line(z, k)
        meta_in.append(remote(meta.at[z], meta.at[z], meta.at[frm], msem, (k - 1,), zdev(to)))
    for g in range(NG):
        for k in LINEK:
            to, frm = line(z, k)
            x_in[g].append(remote(x4[g].at[toks_of(z)], x4[g].at[toks_of(z)], x4[g].at[toks_of(frm)], xsem, (g, k - 1), zdev(to)))

    for m in meta_in:
        m.wait_recv()
    peer = lax.broadcasted_iota(jnp.int32, (PEERS, TOK), 0)
    other = peer >= 16
    here = (z * PEERS + jnp.where(other, peer - 16, peer) * 2 + jnp.where(other, 1 - c, c)).astype(F32)
    before = (
        lax.broadcasted_iota(jnp.int32, (TOK, TOK), 0) < lax.broadcasted_iota(jnp.int32, (TOK, TOK), 1)
    ).astype(F32).astype(BF16)
    wvals, slots, whichs = [], [], []
    for q in range(LINE):
        hit = jnp.zeros((PEERS, TOK), F32)
        wv = jnp.zeros((PEERS, TOK), F32)
        bit = jnp.zeros((PEERS, TOK), F32)
        for k in range(4):
            e = meta[q, k:k + 1, :]
            dev = jnp.floor(e * 0.5)
            is_k = (here == dev).astype(F32)
            hit = hit + is_k
            wv = wv + is_k * meta[q, 4 + k:5 + k, :]
            bit = bit + is_k * (e - 2.0 * dev)
        rank = dot(hit.astype(BF16), before)
        slots.append(jnp.where(hit > 0.0, rank + (8.0 * q + 1.0), 0.0))
        wvals.append(wv)
        whichs.append(bit)

    pad = jnp.zeros((128 - PEERS, TOK), F32)
    for q in range(LINE):
        cut = slice(q * TOK, (q + 1) * TOK)
        vmat[:, cut] = jnp.concatenate([slots[q], pad], axis=0).astype(BF16)

    for m in slab_1:
        m.wait_recv()
    for k in LINEK:
        to, frm = line(x, k)
        slab_2.append(remote(sown.at[x, :, :, top], sown.at[x, :, :, top], sown.at[frm, :, :, top], ssem, (5 + k,), pdev(y, to, c)))
        to, frm = line(y, k)
        slab_2.append(remote(sown.at[:, y, :, low], sown.at[:, y, :, low], sown.at[:, frm, :, low], ssem, (8 + k,), pdev(to, x, c)))

    def sel_tile(i, carry):
        peer, _, target = row_pattern((128, 128), 0, i * 128)
        pick = (peer == lax.broadcasted_iota(jnp.int32, (128, 128), 1).astype(F32)).astype(F32).astype(BF16)
        val = dot(pick, vmat[...])
        sel[pl.ds(pl.multiple_of(i * 128, 128), 128), :] = (val == target[:, 0:1]).astype(F32).astype(BF16)
        return carry

    lax.fori_loop(0, ROWS // 128, sel_tile, 0)

    def dispatch(g):
        for m in x_in[g]:
            m.wait_recv()
        send[g][...] = dot(sel[...], x4[g][...]).astype(BF16)
        return exchange(send, got, g, 0, dsem)

    got_in = [[], []]
    for g in range(EARLY):
        got_in[0].append(dispatch(g))
        got_in[1].append(exchange(send, got, g, 1, dsem))
    got_in[0].append(dispatch(EARLY))

    lane = lax.broadcasted_iota(jnp.int32, (PEERS, 128), 1)
    labels = jnp.zeros((PEERS, 128), F32)
    for q in range(LINE):
        for s in range(CAP):
            bit = jnp.sum(jnp.where(slots[q] == 8.0 * q + s + 1.0, whichs[q], 0.0), axis=1, keepdims=True)
            labels = jnp.where(lane == q * CAP + s, bit, labels)
    for b in range(PEERS):
        lab_out[b] = labels[b:b + 1, :]
    lab_in[spot] = lab_out[spot]
    for h in range(2):
        for to, dev in plane[h]:
            copy_to(lab_out.at[to], lab_in.at[h * 16 + spot], lsem, (), dev).start()
    every = pl.ds(0, len(everyone))
    label_in = copy_to(lab_out.at[every], lab_in.at[every], lsem, (), everyone[0][1])
    sends.append(label_in)
    for q in range(LINE):
        cut = slice(q * TOK, (q + 1) * TOK)
        bits[0, cut, :] = jnp.transpose(jnp.concatenate([slots[q], pad], axis=0)).astype(BF16)
        bits[1, cut, :] = jnp.transpose(jnp.concatenate([wvals[q], pad], axis=0)).astype(BF16)

    for g in range(EARLY + 1, NG):
        got_in[0].append(dispatch(g))
    for g in range(EARLY, NG):
        got_in[1].append(exchange(send, got, g, 1, dsem))
    for m in slab_2:
        m.wait_recv()
    for k in LINEK:
        to, frm = line(z, k)
        slab_z.append(remote(sown.at[:, :, to], sgather.at[c, z], sgather.at[c, frm], ssem, (11 + k,), zdev(to)))
    sgather[c, z] = sown[:, :, z]

    def wsel_tile(i, carry):
        peer, _, target = row_pattern((128, 128), 1, i * 128)
        pick = (peer == lax.broadcasted_iota(jnp.int32, (128, 128), 0).astype(F32)).astype(F32).astype(BF16)
        val = dot(bits[0], pick)
        w = dot(bits[1], pick)
        wsel[:, pl.ds(pl.multiple_of(i * 128, 128), 128)] = jnp.where(val == target[0:1, :], w, 0.0).astype(BF16)
        return carry

    lax.fori_loop(0, ROWS // 128, wsel_tile, 0)

    for w in weights:
        w.wait()
    label_in.wait_recv()
    for b in range(PEERS):
        bits[2, b:b + 1, :] = lab_in[b].astype(BF16)
    peer, inner, _ = row_pattern((ROWS, 128), 0, 0)
    lane = lax.broadcasted_iota(jnp.int32, (ROWS, 128), 1).astype(F32)
    pick = (peer == lane).astype(F32)
    lab = dot(pick.astype(BF16)[:, 0:PEERS], bits[2, 0:PEERS, :])
    which = jnp.sum(jnp.where(inner == lane, lab, 0.0), axis=1, keepdims=True)

    def experts(h):
        rows = slice(h * HALF, (h + 1) * HALF)

        def partial(groups, q, cut):
            return sum(dot(got[g][rows, :], wgu[q, SPANS[g], cut]) for g in groups)

        for n, groups in enumerate(SETS[:-1]):
            for g in groups:
                got_in[h][g].wait_recv()

            def accumulate(q, carry, n=n, groups=groups):
                prod = partial(groups, q, slice(None))
                if n == 0:
                    gu[q, rows, :] = prod
                else:
                    gu[q, rows, :] += prod
                return carry

            lax.fori_loop(0, 4, accumulate, 0)

        for g in SETS[-1]:
            got_in[h][g].wait_recv()
        for e in range(2):
            keep = which[rows] if e == 1 else 1.0 - which[rows]
            for n in range(2):
                cut = slice(n * 256, (n + 1) * 256)
                g = gu[2 * e, rows, cut] + partial(SETS[-1], 2 * e, cut)
                u = gu[2 * e + 1, rows, cut] + partial(SETS[-1], 2 * e + 1, cut)
                hid[rows, e * DE + n * 256:e * DE + (n + 1) * 256] = (silu(g) * u * keep).astype(BF16)

    ret_in = [[] for _ in range(NG)]

    def give_back(g, h):
        rows = slice(h * HALF, (h + 1) * HALF)
        back[g][rows, :] = dot(hid[rows, :], wd[:, SPANS[g]]).astype(BF16)
        ret_in[g].append(exchange(back, ret, g, h, rsem))

    experts(0)
    for g in range(HEAD):
        give_back(g, 0)
    experts(1)
    for g in range(HEAD):
        give_back(g, 1)
    for g in range(HEAD, NG):
        give_back(g, 0)
        give_back(g, 1)

    for m in slab_z:
        m.wait_recv()
    slab_c = remote(sgather.at[c], sgather.at[c], sgather.at[1 - c], ssem, (15,), pdev(y, x, 1 - c))
    slab_c.wait_recv()
    for zz in range(4):
        for yy in range(4):
            for xx in range(4):
                for cc in range(2):
                    r = (((zz * 4 + yy) * 4 + xx) * 2 + cc) * SLAB
                    wsg[r:r + SLAB, :] = sgather[cc, zz, xx, yy, 0:SLAB, :]
                    wsu[r:r + SLAB, :] = sgather[cc, zz, xx, yy, SLAB:2 * SLAB, :]
                    wsd[r:r + SLAB, :] = sgather[cc, zz, xx, yy, 2 * SLAB:3 * SLAB, :]
    g = jnp.zeros((COLS, HS), F32)
    u = jnp.zeros((COLS, HS), F32)
    for q in range(NG):
        g = g + dot(x4[q][...], wsg[SPANS[q], :])
        u = u + dot(x4[q][...], wsu[SPANS[q], :])
    hs[...] = (silu(g) * u).astype(BF16)

    part_in = []
    for g in range(NG):
        for m in ret_in[g]:
            m.wait_recv()
        part[g][...] = (dot(wsel[...], ret[g][...]) + dot_t(hs[...], wsd[SPANS[g], :])).astype(BF16)
        arrivals = []
        for k in LINEK:
            to, frm = line(z, k)
            arrivals.append(remote(part[g].at[toks_of(to)], parts[g].at[toks_of(z)], parts[g].at[toks_of(frm)], psem, (g, k - 1), zdev(to)))
        parts[g][toks_of(z), :] = part[g][toks_of(z), :]
        part_in.append(arrivals)

    stores = []
    for g in range(NG):
        for m in part_in[g]:
            m.wait_recv()
        total = parts[g][0:TOK, :].astype(F32)
        for k in range(1, LINE):
            total = total + parts[g][k * TOK:(k + 1) * TOK, :].astype(F32)
        out[:, SPANS[g]] = total.astype(BF16)
        stores.append(pltpu.make_async_copy(out.at[:, SPANS[g]], out_hbm.at[:, SPANS[g]], osem.at[g]))
        stores[-1].start()

    for s in sends:
        s.wait_send()
    for s in stores:
        s.wait()


def per_device(tokens, norm_gain, expert_ids, gate_weights, expert_gate, expert_up, expert_down, shared_gate, shared_up, shared_down):
    hbm = pl.BlockSpec(memory_space=pl.ANY)
    dma = pltpu.SemaphoreType.DMA

    def per_group(rows):
        return [pltpu.VMEM((rows, f), BF16) for f in SIZES]

    return pl.pallas_call(
        kernel,
        out_shape=jax.ShapeDtypeStruct((TOK, D), BF16),
        in_specs=[hbm] * 10,
        out_specs=hbm,
        scratch_shapes=[
            pltpu.VMEM((TOK, D), BF16),
            pltpu.VMEM((1, D), F32),
            pltpu.VMEM((4, TOK), jnp.int32),
            pltpu.VMEM((4, TOK), F32),
            pltpu.VMEM((SLAB, 4 * HS), BF16),
            pltpu.VMEM((SLAB, 4 * HS), BF16),
            pltpu.VMEM((SLAB, 4 * HS), BF16),
            pltpu.VMEM((4, D, DE), BF16),
            pltpu.VMEM((2 * DE, D), BF16),
            per_group(COLS),
            pltpu.VMEM((LINE, 8, TOK), F32),
            pltpu.VMEM((4, 4, 4, 3 * SLAB, HS), BF16),
            pltpu.VMEM((2, 4, 4, 4, 3 * SLAB, HS), BF16),
            pltpu.VMEM((D, HS), BF16),
            pltpu.VMEM((D, HS), BF16),
            pltpu.VMEM((D, HS), BF16),
            pltpu.VMEM((128, COLS), BF16),
            pltpu.VMEM((3, COLS, 128), BF16),
            pltpu.VMEM((ROWS, COLS), BF16),
            pltpu.VMEM((COLS, ROWS), BF16),
            pltpu.VMEM((PEERS, 1, 128), F32),
            pltpu.VMEM((PEERS, 1, 128), F32),
            per_group(ROWS),
            per_group(ROWS),
            pltpu.VMEM((4, ROWS, DE), F32),
            pltpu.VMEM((ROWS, 2 * DE), BF16),
            per_group(ROWS),
            per_group(ROWS),
            pltpu.VMEM((COLS, HS), BF16),
            per_group(COLS),
            per_group(COLS),
            pltpu.VMEM((TOK, D), BF16),
            dma((7,)),
            dma((6,)),
            dma((NG,)),
            dma((2, 3)),
            dma((2, 16)),
            dma((2, NG, 3)),
            dma((2,)),
            dma((2, NG, 2)),
            dma((2, NG, 2)),
            dma((2, NG, 3)),
        ],
        compiler_params=pltpu.CompilerParams(
            collective_id=0, has_side_effects=True, vmem_limit_bytes=67043328
        ),
        name="moe",
    )(
        tokens, norm_gain.reshape(1, D), expert_ids.T, gate_weights.T,
        shared_gate, shared_up, shared_down.T, expert_gate, expert_up, expert_down,
    )


def solution(mesh):
    ep = P("ep")
    return jax.shard_map(
        per_device,
        mesh=mesh,
        in_specs=(ep, P(), ep, ep, ep, ep, ep, ep, ep, P(None, "ep")),
        out_specs=ep,
        check_vma=False,
    )
```

time: 105 us -> 99.9 us (0.951)
  Pallas kernels: 102 us -> 97.9 us
    pallas_call x1, Pallas kernels: 102 us -> 97.9 us  [per_device(): pl.pallas_call(kernel, out_shape=jax.ShapeDtypeStruct((TOK, D), BF16), in...]
where the time goes in v3:
time: 99.9 us; the launch traced here: 99.8 us
  Pallas kernels  97.9 us (98%)
  local copies, waits for them, and re-layouts  1.88 us (2%)
    pallas_call x1, Pallas kernels, per_device(): pl.pallas_call(kernel, out_shape=jax.ShapeDtypeStruct((TOK, D), BF16), in...  97.9 us

profile of v3, /device:TPU:1, one launch (start us, length us, event | category | flops | bytes accessed | tf_op | source)
XLA Modules:
  0.0 99.8 jit_solution(11510240689773095674)
XLA Ops:
  0.0 97.9 %moe.1 = bf16[128,2048]{1,0:T(8,128)(2,1)} custom-call(bf16[128,2048]{1,0:T(8,128)(2,1)} %tok_hbm.1, f32[1,2048]{1,0:T(1,128)} %bitcast.5, s32[4,128]{1,0:T(4,128)} %bitcast.6, f32[4,128]{1,0:T(4,128)} %bitcast.7, bf16[16,512]{1,0:T(8,128)(2,1)} %sg_hbm.1, bf16[16,512]{1,0:T(8,128)(2,1)} %su_hbm.1, bf16[16,512]{1,0:T(8,128)(2,1)} %bitcast.4, ...), custom_call_target="tpu_custom_call" | custom-call | tf_op jit(solution)/shard_map/moe/pallas_call | solution.py:390
  97.9 1.9 %copy.12 = bf16[128,2048]{1,0:T(8,128)(2,1)} copy(bf16[128,2048]{1,0:T(8,128)(2,1)} %moe.1) | data formatting | bytes 1048576

commit v4 on v3

--- a/solution.py
+++ b/solution.py
@@ -11,7 +11,7 @@
 
 D = 2048
 DE = 512
-SIZES = [256, 512, 512, 512, 256]
+SIZES = [256, 512, 512, 384, 384]
 NG = len(SIZES)
 SETS = [[0, 1], [2, 3], [4]]
 SPANS = [slice(sum(SIZES[:g]), sum(SIZES[:g + 1])) for g in range(NG)]

time: 99.9 us -> 98.6 us (0.987)
  Pallas kernels: 97.9 us -> 96.6 us
    pallas_call x1, Pallas kernels: 97.9 us -> 96.6 us  [per_device(): pl.pallas_call(kernel, out_shape=jax.ShapeDtypeStruct((TOK, D), BF16), in...]
where the time goes in v4:
time: 98.6 us; the launch traced here: 98.5 us
  Pallas kernels  96.6 us (98%)
  local copies, waits for them, and re-layouts  1.88 us (2%)
    pallas_call x1, Pallas kernels, per_device(): pl.pallas_call(kernel, out_shape=jax.ShapeDtypeStruct((TOK, D), BF16), in...  96.6 us

profile of v4, /device:TPU:1, one launch (start us, length us, event | category | flops | bytes accessed | tf_op | source)
XLA Modules:
  0.0 98.5 jit_solution(17546220008633443445)
XLA Ops:
  0.0 96.6 %moe.1 = bf16[128,2048]{1,0:T(8,128)(2,1)} custom-call(bf16[128,2048]{1,0:T(8,128)(2,1)} %tok_hbm.1, f32[1,2048]{1,0:T(1,128)} %bitcast.5, s32[4,128]{1,0:T(4,128)} %bitcast.6, f32[4,128]{1,0:T(4,128)} %bitcast.7, bf16[16,512]{1,0:T(8,128)(2,1)} %sg_hbm.1, bf16[16,512]{1,0:T(8,128)(2,1)} %su_hbm.1, bf16[16,512]{1,0:T(8,128)(2,1)} %bitcast.4, ...), custom_call_target="tpu_custom_call" | custom-call | tf_op jit(solution)/shard_map/moe/pallas_call | solution.py:390
  96.6 1.9 %copy.12 = bf16[128,2048]{1,0:T(8,128)(2,1)} copy(bf16[128,2048]{1,0:T(8,128)(2,1)} %moe.1) | data formatting | bytes 1048576
